TPU v7x, 32 devices: a whole 2x2x4 slice. The times are simulated.
32 devices in a mesh: sp: 16 (over z, y, x), tp: 2 (over core).
Axes of the slice: x: 2, y: 2, z: 4, core: 2. Of those that a mesh axis runs over, the one named last changes fastest.
Arguments:
- queries: bfloat16 [8192, 2048], P('sp', 'tp'), may hold values from -6 to 6
- key_rows: bfloat16 [8192, 512], P('sp', 'tp'), may hold values from -6 to 6
- values: bfloat16 [8192, 512], P('sp', 'tp'), may hold values from -6 to 6
- sink_logit: float32 [32], P('tp'), may hold values from 4 to 10
- residual_in: bfloat16 [8192, 2048], P(('sp', 'tp')), may hold values from -6 to 6
- out_weight: bfloat16 [2048, 2048], P('tp'), may hold values from -0.125 to 0.125
- norm_gain: float32 [2048], replicated, may hold values from 0.1 to 1.9
- gate_weight: bfloat16 [2048, 5632], P('sp', 'tp'), may hold values from -0.125 to 0.125
- up_weight: bfloat16 [2048, 5632], P('sp', 'tp'), may hold values from -0.125 to 0.125
- down_weight: bfloat16 [5632, 2048], P('tp', 'sp'), may hold values from -0.078125 to 0.078125
Outputs:
- layer_out: bfloat16 [8192, 2048], P(('sp', 'tp'))
All inputs are finite; a program needn't handle non-finite values.
Results may differ from a plain program's by a relative error of at most 0.013.
Values may be sent and summed in bfloat16 or wider, within the bound.
A program may use at most 128 MiB of HBM per device.

v0:
```python
import jax
import jax.numpy as jnp
from jax import lax
from jax.sharding import PartitionSpec as P

HEAD_DIM = 64
WINDOW = 128


def with_halo(block, sides, width):
    for axis, dim in sides:
        count = lax.axis_size(axis)
        forward = [(i, i + 1) for i in range(count - 1)]
        backward = [(target, source) for source, target in forward]
        low = lax.ppermute(
            lax.slice_in_dim(block, block.shape[dim] - width, None, axis=dim), axis, forward
        )
        high = lax.ppermute(lax.slice_in_dim(block, 0, width, axis=dim), axis, backward)
        block = jnp.concatenate([low, block, high], axis=dim)
    return block


def rms_scale(mixed_rows, norm_gain):
    inverse = lax.rsqrt(jnp.mean(mixed_rows * mixed_rows, axis=-1, keepdims=True) + 1e-06)
    return (mixed_rows * inverse * norm_gain).astype(jnp.bfloat16)


def attend_window(queries, padded, offset, total_rows, sink_logit):
    rows_here = queries.shape[0]
    block_count = rows_here // WINDOW
    heads_here = queries.shape[1] // HEAD_DIM
    kv_here = padded.shape[1] // (2 * HEAD_DIM)
    group_size = heads_here // kv_here
    blocks = padded.reshape(block_count + 2, WINDOW, padded.shape[1])
    banded = jnp.concatenate([blocks[:-2], blocks[1:-1], blocks[2:]], axis=1)
    key_band = banded[:, :, : kv_here * HEAD_DIM].reshape(
        block_count, 3 * WINDOW, kv_here, HEAD_DIM
    )
    value_band = banded[:, :, kv_here * HEAD_DIM :].reshape(
        block_count, 3 * WINDOW, kv_here, HEAD_DIM
    )
    grouped = queries.reshape(block_count, WINDOW, kv_here, group_size, HEAD_DIM)
    scores = jnp.einsum(
        "nqkgd,nskd->nkgqs", grouped, key_band, preferred_element_type=jnp.float32
    ) * HEAD_DIM ** (-0.5)
    block_start = offset + jnp.arange(block_count, dtype=jnp.int32)[:, None] * WINDOW
    query_pos = block_start + jnp.arange(WINDOW, dtype=jnp.int32)[None, :]
    key_pos = block_start - WINDOW + jnp.arange(3 * WINDOW, dtype=jnp.int32)[None, :]
    valid = jnp.abs(query_pos[:, :, None] - key_pos[:, None, :]) <= WINDOW
    valid = valid & ((key_pos >= 0) & (key_pos < total_rows))[:, None, :]
    scores = jnp.where(valid[:, None, None], scores, -1e30)
    sink_grid = sink_logit.reshape(kv_here, group_size)[None, :, :, None, None]
    peak = jnp.maximum(jnp.max(scores, axis=-1, keepdims=True), sink_grid)
    weights_raw = jnp.exp(scores - peak)
    denom = jnp.sum(weights_raw, axis=-1, keepdims=True) + jnp.exp(sink_grid - peak)
    probs = (weights_raw / denom).astype(jnp.bfloat16)
    output = jnp.einsum("nkgqs,nskd->nqkgd", probs, value_band, preferred_element_type=jnp.float32)
    return output.astype(jnp.bfloat16).reshape(rows_here, heads_here * HEAD_DIM)


def shards(
    queries,
    key_rows,
    values,
    sink_logit,
    residual_in,
    out_weight,
    norm_gain,
    gate_weight,
    up_weight,
    down_weight,
):
    rows_here = queries.shape[0]
    row_share = rows_here // lax.axis_size("tp")
    joined = jnp.concatenate([key_rows, values], axis=1)
    padded = with_halo(joined, (("sp", 0),), WINDOW)
    offset = lax.axis_index("sp") * rows_here
    attended = attend_window(queries, padded, offset, rows_here * lax.axis_size("sp"), sink_logit)
    partial_value = jnp.dot(attended, out_weight, preferred_element_type=jnp.float32)
    summed = lax.psum(partial_value.astype(jnp.bfloat16), "tp").astype(jnp.float32)
    whole_residual = lax.all_gather(residual_in, "tp", axis=0, tiled=True)
    mixed_whole = whole_residual.astype(jnp.float32) + summed
    normed = rms_scale(mixed_whole, norm_gain)
    mixed_rows = lax.dynamic_slice_in_dim(
        mixed_whole, lax.axis_index("tp") * row_share, row_share, 0
    )
    gate_full, up_full = (
        lax.all_gather(gate_weight, "sp", axis=0, tiled=True),
        lax.all_gather(up_weight, "sp", axis=0, tiled=True),
    )
    down_full = lax.all_gather(down_weight, "sp", axis=1, tiled=True)
    gate_pre = jnp.dot(normed, gate_full, preferred_element_type=jnp.float32)
    up_pre = jnp.dot(normed, up_full, preferred_element_type=jnp.float32)
    hidden = (jax.nn.silu(gate_pre) * up_pre).astype(jnp.bfloat16)
    result = mixed_rows + lax.psum_scatter(
        jnp.dot(hidden, down_full, preferred_element_type=jnp.float32).astype(jnp.bfloat16),
        "tp",
        scatter_dimension=0,
        tiled=True,
    ).astype(jnp.float32)
    return result.astype(jnp.bfloat16)


def solution(mesh):
    return jax.shard_map(
        shards,
        mesh=mesh,
        in_specs=(
            P("sp", "tp"),
            P("sp", "tp"),
            P("sp", "tp"),
            P("tp"),
            P(("sp", "tp"), None),
            P("tp", None),
            P(),
            P("sp", "tp"),
            P("sp", "tp"),
            P("tp", "sp"),
        ),
        out_specs=P(("sp", "tp"), None),
        check_vma=False,
    )
```

profile of v0, /device:TPU:0, one launch (start us, length us, event | category | flops | bytes accessed | tf_op | source)
XLA Modules:
  0.0 577.9 jit_solution(7565747926765776180)
XLA Ops:
  6.5 1.0 constant_dynamic-update-slice_fusion.1
  7.5 1.0 constant_dynamic-update-slice_fusion
  8.5 4.9 collective-permute-start
  13.4 1.3 collective-permute-start.1
  14.9 1.0 copy.17
  16.0 4.1 reshape.117
  20.2 0.1 max.18
  20.3 0.6 fusion.9
  20.8 0.1 collective-permute-done.1
  21.0 1.8 pad_maximum_fusion.2
  22.8 1.4 copy.16
  24.1 1.0 copy.18
  25.1 1.5 pad_maximum_fusion
  26.6 0.2 fusion.14
  26.8 2.5 fusion.1
  29.4 3.4 fusion
  32.7 0.1 exponential_add_fusion
  32.9 3.8 fusion.6
  36.6 0.9 copy.22
  37.5 3.8 convolution_convert_fusion
  41.4 0.7 all-gather.7.cloned.1.call-update
  42.2 0.5 all-gather.11.cloned.1.call-update
  42.8 0.5 all-gather.9.cloned.1.call-update
  43.4 22.3 %all-reduce.2.cloned.1.call-done = bf16[512,2048]{1,0:T(8,128)(2,1)} async-done(((bf16[512,2048]{1,0:T(8,128)(2,1)}), bf16[512,2048]{1,0:T(8,128)(2,1)}) %all-reduce.2.cloned.1.call-update) | async-done | bytes 2097168 | tf_op jit(solution)/shard_map/psum | solution.py:80
  65.7 4.9 convert_add_fusion
  70.6 140.5 %all-gather.7.cloned.1.call-done = bf16[2048,2816]{1,0:T(8,128)(2,1)} async-done(((bf16[128,2816]{1,0:T(8,128)(2,1)}), bf16[2048,2816]{1,0:T(8,128)(2,1)}) %all-gather.7.cloned.1.call-update) | async-done | bytes 11534352 | tf_op jit(solution)/shard_map/all_gather | solution.py:88
  211.1 12.8 %fusion.13 = f32[512,2816]{1,0:T(8,128)} fusion(bf16[2048,2816]{1,0:T(8,128)(2,1)} %all-gather.7.cloned.1.call-done, f32[2048]{0:T(1024)S(1)} %copy-done.3, f32[512]{0:T(512)S(1)} %add_rsqrt_fusion, bf16[512,2048]{1,0:T(8,128)(2,1)} %all-reduce.2.cloned.1.call-done, bf16[512,2048]{1,0:T(8,128)(2,1)S(1)} %copy-done), kind=kOutput, calls=%fused_computation.37 | convolution fusion | flops 5911871488 | bytes 21506048 | tf_op jit(solution)/shard_map/dot_general | solution.py:92
  223.9 170.0 %all-gather.11.cloned.1.call-done = bf16[2816,2048]{1,0:T(8,128)(2,1)} async-done(((bf16[2816,128]{1,0:T(8,128)(2,1)}), bf16[2816,2048]{1,0:T(8,128)(2,1)}) %all-gather.11.cloned.1.call-update) | async-done | bytes 11534352 | tf_op jit(solution)/shard_map/all_gather | solution.py:91
  393.9 142.2 %all-gather.9.cloned.1.call-done = bf16[2048,2816]{1,0:T(8,128)(2,1)} async-done(((bf16[128,2816]{1,0:T(8,128)(2,1)}), bf16[2048,2816]{1,0:T(8,128)(2,1)}) %all-gather.9.cloned.1.call-update) | async-done | bytes 11534352 | tf_op jit(solution)/shard_map/all_gather | solution.py:89
  536.1 23.6 %convolution_convert_fusion.1 = bf16[512,2048]{1,0:T(8,128)(2,1)} fusion(bf16[2816,2048]{1,0:T(8,128)(2,1)} %all-gather.11.cloned.1.call-done, f32[512,2816]{1,0:T(8,128)} %fusion.13, bf16[2048,2816]{1,0:T(8,128)(2,1)} %all-gather.9.cloned.1.call-done, f32[2048]{0:T(1024)S(1)} %copy-done.3, f32[512]{0:T(512)S(1)} %add_rsqrt_fusion, ...), kind=kOutput, calls=%fused_computation.11 | convolution fusion | flops 11827150848 | bytes 35137536 | tf_op jit(solution)/shard_map/dot_general | solution.py:96
  559.7 8.1 %reduce-scatter.2.cloned.1.call-done = bf16[256,2048]{1,0:T(8,128)(2,1)} async-done(((bf16[512,2048]{1,0:T(8,128)(2,1)}), bf16[256,2048]{1,0:T(8,128)(2,1)}) %reduce-scatter.2.cloned.1.call-update) | async-done | bytes 1048592 | tf_op jit(solution)/shard_map/reduce_scatter | solution.py:95
  567.8 3.2 add_convert_fusion
  (26 shorter events, 0.6 us)
Async XLA Ops:
  6.5 13.6 %copy-start.1 = (f32[16]{0:T(128)S(1)}, f32[16]{0:T(128)}, u32[]{:S(2)}) copy-start(f32[16]{0:T(128)} %param.13) | copy-start | bytes 196
  6.5 36.8 %all-gather.5.cloned.1.call-start = ((), (), s32[]{:S(2)}) async-start(), calls=%async_computation.1 | async-start | bytes 3145728 | tf_op jit(solution)/shard_map/all_gather | solution.py:81
  8.5 12.3 %collective-permute-start = (bf16[128,512]{1,0:T(8,128)(2,1)S(1)}, bf16[128,512]{1,0:T(8,128)(2,1)S(1)}, u32[]{:S(2)}, u32[]{:S(2)}) collective-permute-start(bf16[128,512]{1,0:T(8,128)(2,1)S(1)} %get-tuple-element.11), channel_id=1, source_target_pairs={{0,2},{2,4},{4,6},{6,8},{8,10},{10,12},{12,14},{14,16},{16,18},{18... | collective-permute-start | bytes 393224 | tf_op jit(solution)/shard_map/ppermute | solution.py:15
  13.4 7.6 %collective-permute-start.1 = (bf16[128,512]{1,0:T(8,128)(2,1)S(1)}, bf16[128,512]{1,0:T(8,128)(2,1)}, u32[]{:S(2)}, u32[]{:S(2)}) collective-permute-start(bf16[128,512]{1,0:T(8,128)(2,1)S(1)} %get-tuple-element.12), channel_id=1, source_target_pairs={{2,0},{4,2},{6,4},{8,6},{10,8},{12,10},{14,12},{16,14},{18,16},{20... | collective-permute-start | bytes 393224 | tf_op jit(solution)/shard_map/ppermute | solution.py:18
  14.7 50.9 %all-reduce.2.cloned.1.call-start = ((), (), s32[]{:S(2)}) async-start(), calls=%async_computation.2 | async-start | bytes 4194304 | tf_op jit(solution)/shard_map/psum | solution.py:80
  32.8 4.7 copy-start.2
  41.4 169.7 %all-gather.7.cloned.1.call-start = ((), (), s32[]{:S(2)}) async-start(), calls=%async_computation.3 | async-start | bytes 12255232 | tf_op jit(solution)/shard_map/all_gather | solution.py:88
  42.1 351.7 %all-gather.11.cloned.1.call-start = ((), (), s32[]{:S(2)}) async-start(), calls=%async_computation.5 | async-start | bytes 12255232 | tf_op jit(solution)/shard_map/all_gather | solution.py:91
  42.7 493.4 %all-gather.9.cloned.1.call-start = ((), (), s32[]{:S(2)}) async-start(), calls=%async_computation.4 | async-start | bytes 12255232 | tf_op jit(solution)/shard_map/all_gather | solution.py:89
  43.3 167.8 %copy-start.3 = (f32[2048]{0:T(1024)S(1)}, f32[2048]{0:T(1024)}, u32[]{:S(2)}) copy-start(f32[2048]{0:T(1024)} %param.16) | copy-start | bytes 24580
  43.3 524.5 %reduce-scatter.2.cloned.1.call-start = ((), (), s32[]{:S(2)}) async-start(), calls=%async_computation.6 | async-start | bytes 3145728 | tf_op jit(solution)/shard_map/reduce_scatter | solution.py:95
  43.4 167.7 %copy-start = (bf16[512,2048]{1,0:T(8,128)(2,1)S(1)}, bf16[512,2048]{1,0:T(8,128)(2,1)}, u32[]{:S(2)}) copy-start(bf16[512,2048]{1,0:T(8,128)(2,1)} %all-gather.5.cloned.1.call-done) | copy-start | bytes 6291460
Sparse Core Ops, SparseCore 0:
  14.9 13.6 all-gather.4
  41.5 24.0 all-reduce.1
  68.4 142.5 all-gather.6
  213.6 180.2 all-gather.10
  396.5 139.5 all-gather.8
  559.9 7.9 reduce-scatter.1
where the time goes:
time: 578 us
  waiting for transfers between devices  485 us (84%)
  matrix products  46.6 us (8%)
  other arithmetic  15.7 us (3%)
  between operations  13.6 us (2%)
  local copies, waits for them, and re-layouts  10.6 us (2%)
  starting transfers between devices  6.37 us (1%)
    all_gather x1, waiting for transfers between devices, shards(): down_full = lax.all_gather(down_weight, 'sp', axis=1, tiled=True)  170 us
    all_gather x1, waiting for transfers between devices, shards(): lax.all_gather(up_weight, 'sp', axis=0, tiled=True)  142 us
    all_gather x1, waiting for transfers between devices, shards(): lax.all_gather(gate_weight, 'sp', axis=0, tiled=True)  141 us
    dot_general x1, matrix products, shards(): jnp.dot(hidden, down_full, preferred_element_type=jnp.float32)  23.6 us
    psum x1, waiting for transfers between devices, shards(): lax.psum(partial_value.astype(jnp.bfloat16), 'tp').astype(jnp.float32)  22.3 us
    dot_general x1, matrix products, shards(): gate_pre = jnp.dot(normed, gate_full, preferred_element_type=jnp.float32)  12.8 us
  transfers between devices with their start and end apart: 8, of which 6 were waited for; matrix products, arithmetic and copies ran while one was open for 8% of the time, Pallas kernels for 0%

commit v1 on v0

--- a/solution.py
+++ b/solution.py
@@ -88,7 +88,7 @@
         lax.all_gather(gate_weight, "sp", axis=0, tiled=True),
         lax.all_gather(up_weight, "sp", axis=0, tiled=True),
     )
-    down_full = lax.all_gather(down_weight, "sp", axis=1, tiled=True)
+    down_full = jnp.concatenate(lax.all_gather(down_weight, "sp"), axis=1)
     gate_pre = jnp.dot(normed, gate_full, preferred_element_type=jnp.float32)
     up_pre = jnp.dot(normed, up_full, preferred_element_type=jnp.float32)
     hidden = (jax.nn.silu(gate_pre) * up_pre).astype(jnp.bfloat16)

time: 578 us -> 542 us (0.938)
  waiting for transfers between devices: 485 us -> 429 us
  local copies, waits for them, and re-layouts: 10.6 us -> 26 us
    all_gather x1, waiting for transfers between devices: 170 us -> 141 us  [shards(): down_full = jnp.concatenate(lax.all_gather(down_weight, 'sp'), axis=1)]
    reshape x0 -> x1, local copies, waits for them, and re-layouts: none -> 15.4 us  [shards(): down_full = jnp.concatenate(lax.all_gather(down_weight, 'sp'), axis=1)]
    all_gather x1, waiting for transfers between devices: 141 us -> 127 us  [shards(): lax.all_gather(gate_weight, 'sp', axis=0, tiled=True)]
    all_gather x1, waiting for transfers between devices: 142 us -> 129 us  [shards(): lax.all_gather(up_weight, 'sp', axis=0, tiled=True)]
  transfers between devices with their start and end apart: 8 -> 8, of which waited for: 6 -> 6; matrix products, arithmetic and copies ran while one was open for 8% -> 11% of each run, Pallas kernels for 0% -> 0%
where the time goes in v1:
time: 542 us; the launch traced here: 541 us
  waiting for transfers between devices  429 us (79%)
  matrix products  50.4 us (9%)
  local copies, waits for them, and re-layouts  26 us (5%)
  other arithmetic  15.6 us (3%)
  between operations  13.6 us (3%)
  starting transfers between devices  6.37 us (1%)
    all_gather x1, waiting for transfers between devices, shards(): down_full = jnp.concatenate(lax.all_gather(down_weight, 'sp'), axis=1)  141 us
    all_gather x1, waiting for transfers between devices, shards(): lax.all_gather(up_weight, 'sp', axis=0, tiled=True)  129 us
    all_gather x1, waiting for transfers between devices, shards(): lax.all_gather(gate_weight, 'sp', axis=0, tiled=True)  127 us
    dot_general x1, matrix products, shards(): jnp.dot(hidden, down_full, preferred_element_type=jnp.float32)  27.5 us
    psum x1, waiting for transfers between devices, shards(): lax.psum(partial_value.astype(jnp.bfloat16), 'tp').astype(jnp.float32)  22.3 us
    reshape x1, local copies, waits for them, and re-layouts, shards(): down_full = jnp.concatenate(lax.all_gather(down_weight, 'sp'), axis=1)  15.4 us
    dot_general x1, matrix products, shards(): gate_pre = jnp.dot(normed, gate_full, preferred_element_type=jnp.float32)  12.8 us
  transfers between devices with their start and end apart: 8, of which 6 were waited for; matrix products, arithmetic and copies ran while one was open for 11% of the time, Pallas kernels for 0%

profile of v1, /device:TPU:0, one launch (start us, length us, event | category | flops | bytes accessed | tf_op | source)
XLA Modules:
  0.0 541.1 jit_solution(9308601286852341785)
XLA Ops:
  6.5 1.0 constant_dynamic-update-slice_fusion.1
  7.5 1.0 constant_dynamic-update-slice_fusion
  8.5 4.9 collective-permute-start
  13.4 1.3 collective-permute-start.1
  14.9 1.0 copy.24
  16.0 4.1 reshape.126
  20.3 0.6 fusion.9
  20.8 0.1 collective-permute-done.1
  21.0 1.8 pad_maximum_fusion.2
  22.8 1.4 copy.23
  24.1 1.0 copy.25
  25.1 1.5 pad_maximum_fusion
  26.6 0.2 fusion.14
  26.8 2.5 fusion.1
  29.4 3.4 fusion
  32.7 0.1 exponential_add_fusion
  32.9 3.8 fusion.6
  36.6 0.9 copy.29
  37.5 3.8 convolution_convert_fusion
  41.5 0.7 all-gather.12.cloned.1.call-update
  42.2 0.5 all-gather.8.cloned.1.call-update
  42.8 0.5 all-gather.10.cloned.1.call-update
  43.4 22.3 %all-reduce.2.cloned.1.call-done = bf16[512,2048]{1,0:T(8,128)(2,1)} async-done(((bf16[512,2048]{1,0:T(8,128)(2,1)}), bf16[512,2048]{1,0:T(8,128)(2,1)}) %all-reduce.2.cloned.1.call-update) | async-done | bytes 2097168 | tf_op jit(solution)/shard_map/psum | solution.py:80
  65.7 4.8 convert_add_fusion
  70.5 140.6 %all-gather.12.cloned.1.call-done = bf16[45056,128]{1,0:T(8,128)(2,1)} async-done(((bf16[2816,128]{1,0:T(8,128)(2,1)}), bf16[45056,128]{1,0:T(8,128)(2,1)}) %all-gather.12.cloned.1.call-update) | async-done | bytes 11534352 | tf_op jit(solution)/shard_map/all_gather | solution.py:91
  211.1 15.4 %copy.30 = bf16[2816,16,128]{0,2,1:T(8,128)(2,1)} copy(bf16[2816,16,128]{2,0,1:T(8,128)(2,1)} %bitcast.45) | data formatting | bytes 23068672 | tf_op jit(solution)/shard_map/reshape | solution.py:91
  226.4 126.9 %all-gather.8.cloned.1.call-done = bf16[2048,2816]{1,0:T(8,128)(2,1)} async-done(((bf16[128,2816]{1,0:T(8,128)(2,1)}), bf16[2048,2816]{1,0:T(8,128)(2,1)}) %all-gather.8.cloned.1.call-update) | async-done | bytes 11534352 | tf_op jit(solution)/shard_map/all_gather | solution.py:88
  353.3 12.8 %fusion.13 = f32[512,2816]{1,0:T(8,128)} fusion(bf16[2048,2816]{1,0:T(8,128)(2,1)} %all-gather.8.cloned.1.call-done, f32[2048]{0:T(1024)S(1)} %copy-done.3, f32[512]{0:T(512)S(1)} %add_rsqrt_fusion, bf16[512,2048]{1,0:T(8,128)(2,1)} %all-reduce.2.cloned.1.call-done, bf16[512,2048]{1,0:T(8,128)(2,1)S(1)} %copy-done), kind=kOutput, calls=%fused_computation.37 | convolution fusion | flops 5911871488 | bytes 21506048 | tf_op jit(solution)/shard_map/dot_general | solution.py:92
  366.2 129.4 %all-gather.10.cloned.1.call-done = bf16[2048,2816]{1,0:T(8,128)(2,1)} async-done(((bf16[128,2816]{1,0:T(8,128)(2,1)}), bf16[2048,2816]{1,0:T(8,128)(2,1)}) %all-gather.10.cloned.1.call-update) | async-done | bytes 11534352 | tf_op jit(solution)/shard_map/all_gather | solution.py:89
  495.5 27.5 %convolution_convert_fusion.1 = bf16[512,2048]{1,0:T(8,128)(2,1)} fusion(bf16[2816,2048]{0,1:T(8,128)(2,1)} %bitcast.46, f32[512,2816]{1,0:T(8,128)} %fusion.13, bf16[2048,2816]{1,0:T(8,128)(2,1)} %all-gather.10.cloned.1.call-done, f32[2048]{0:T(1024)S(1)} %copy-done.3, f32[512]{0:T(512)S(1)} %add_rsqrt_fusion, ...), kind=kOutput, calls=%fused_computation.11 | convolution fusion | flops 11827150848 | bytes 35137536 | tf_op jit(solution)/shard_map/dot_general | solution.py:96
  523.0 8.1 %reduce-scatter.2.cloned.1.call-done = bf16[256,2048]{1,0:T(8,128)(2,1)} async-done(((bf16[512,2048]{1,0:T(8,128)(2,1)}), bf16[256,2048]{1,0:T(8,128)(2,1)}) %reduce-scatter.2.cloned.1.call-update) | async-done | bytes 1048592 | tf_op jit(solution)/shard_map/reduce_scatter | solution.py:95
  531.1 3.2 add_convert_fusion
  (27 shorter events, 0.7 us)
Async XLA Ops:
  6.5 13.6 %copy-start.1 = (f32[16]{0:T(128)S(1)}, f32[16]{0:T(128)}, u32[]{:S(2)}) copy-start(f32[16]{0:T(128)} %param.13) | copy-start | bytes 196
  6.5 36.8 %all-gather.6.cloned.1.call-start = ((), (), s32[]{:S(2)}) async-start(), calls=%async_computation.1 | async-start | bytes 3145728 | tf_op jit(solution)/shard_map/all_gather | solution.py:81
  8.5 12.3 %collective-permute-start = (bf16[128,512]{1,0:T(8,128)(2,1)S(1)}, bf16[128,512]{1,0:T(8,128)(2,1)S(1)}, u32[]{:S(2)}, u32[]{:S(2)}) collective-permute-start(bf16[128,512]{1,0:T(8,128)(2,1)S(1)} %get-tuple-element.11), channel_id=1, source_target_pairs={{0,2},{2,4},{4,6},{6,8},{8,10},{10,12},{12,14},{14,16},{16,18},{18... | collective-permute-start | bytes 393224 | tf_op jit(solution)/shard_map/ppermute | solution.py:15
  13.4 7.6 %collective-permute-start.1 = (bf16[128,512]{1,0:T(8,128)(2,1)S(1)}, bf16[128,512]{1,0:T(8,128)(2,1)}, u32[]{:S(2)}, u32[]{:S(2)}) collective-permute-start(bf16[128,512]{1,0:T(8,128)(2,1)S(1)} %get-tuple-element.12), channel_id=1, source_target_pairs={{2,0},{4,2},{6,4},{8,6},{10,8},{12,10},{14,12},{16,14},{18,16},{20... | collective-permute-start | bytes 393224 | tf_op jit(solution)/shard_map/ppermute | solution.py:18
  14.7 50.9 %all-reduce.2.cloned.1.call-start = ((), (), s32[]{:S(2)}) async-start(), calls=%async_computation.2 | async-start | bytes 4194304 | tf_op jit(solution)/shard_map/psum | solution.py:80
  32.8 4.7 copy-start.2
  41.4 169.7 %all-gather.12.cloned.1.call-start = ((), (), s32[]{:S(2)}) async-start(), calls=%async_computation.6 | async-start | bytes 12255232 | tf_op jit(solution)/shard_map/all_gather | solution.py:91
  42.1 311.2 %all-gather.8.cloned.1.call-start = ((), (), s32[]{:S(2)}) async-start(), calls=%async_computation.3 | async-start | bytes 12255232 | tf_op jit(solution)/shard_map/all_gather | solution.py:88
  42.7 452.8 %all-gather.10.cloned.1.call-start = ((), (), s32[]{:S(2)}) async-start(), calls=%async_computation.4 | async-start | bytes 12255232 | tf_op jit(solution)/shard_map/all_gather | solution.py:89
  43.3 487.8 %reduce-scatter.2.cloned.1.call-start = ((), (), s32[]{:S(2)}) async-start(), calls=%async_computation.5 | async-start | bytes 3145728 | tf_op jit(solution)/shard_map/reduce_scatter | solution.py:95
  211.1 142.2 %copy-start = (bf16[512,2048]{1,0:T(8,128)(2,1)S(1)}, bf16[512,2048]{1,0:T(8,128)(2,1)}, u32[]{:S(2)}) copy-start(bf16[512,2048]{1,0:T(8,128)(2,1)} %all-gather.6.cloned.1.call-done) | copy-start | bytes 6291460
  211.1 142.2 %copy-start.3 = (f32[2048]{0:T(1024)S(1)}, f32[2048]{0:T(1024)}, u32[]{:S(2)}) copy-start(f32[2048]{0:T(1024)} %param.16) | copy-start | bytes 24580
Sparse Core Ops, SparseCore 0:
  14.9 13.6 all-gather.5
  41.5 24.0 all-reduce.1
  68.4 142.5 all-gather.11
  213.7 139.5 all-gather.7
  355.9 139.5 all-gather.9
  523.1 7.9 reduce-scatter.1
